TPU v7x, 256 devices: a whole 4x4x8 slice. The times are simulated.
256 devices in a mesh: ep: 64 (over z, y, core), tp: 4 (over x).
Axes of the slice: x: 4, y: 4, z: 8, core: 2. Of those that a mesh axis runs over, the one named last changes fastest.
Arguments:
- query: bfloat16 [8192, 1536], P('ep', 'tp'), may hold values from -136 to 136
- latent: bfloat16 [8192, 512], P(('ep', 'tp')), may hold values from -6 to 6
- rope_key: bfloat16 [8192, 32], P(('ep', 'tp')), may hold values from -6 to 6
- latent_gain: float32 [512], replicated, may hold values from 0.1 to 1.9
- key_up: bfloat16 [512, 1024], P(None, 'tp'), may hold values from -0.25 to 0.25
- value_up: bfloat16 [512, 1024], P(None, 'tp'), may hold values from -2 to 2
- out_proj: bfloat16 [1024, 2048], replicated, may hold values from -0.1875 to 0.1875
- tokens: bfloat16 [16384, 2048], P(('ep', 'tp')), may hold values from -6 to 6
- moe_gain: float32 [2048], replicated, may hold values from 0.1 to 1.9
- routes: int32 [16384, 2], P(('ep', 'tp')), may hold values from 0 to 63, all different within a row; in each aligned block of 64 rows (0 to 63, 64 to 127, ...) at most 4 rows name the same one
- group_prob: float32 [16384], P(('ep', 'tp')), may hold values from 0.25 to 1
- expert_prob: float32 [16384, 2], P(('ep', 'tp')), may hold values from 0.02 to 1
- w_gate: bfloat16 [64, 2048, 1024], P('ep', None, 'tp'), may hold values from -0.125 to 0.125
- w_up: bfloat16 [64, 2048, 1024], P('ep', None, 'tp'), may hold values from -0.125 to 0.125
- w_down: bfloat16 [64, 1024, 2048], P('ep', 'tp'), may hold values from -0.1875 to 0.1875
Outputs:
- mixed: bfloat16 [8192, 2048], P(('ep', 'tp'))
- moe_out: bfloat16 [16384, 2048], P(('ep', 'tp'))
Inputs may be any that keep to these rules, and one draw needn't show every extreme that they name: `routes`: each row names 2 different experts; within the rows of one device no expert is named more than 4 times.
All inputs are finite; a program needn't handle non-finite values.
Results may differ from a plain program's by a relative error of at most 0.025.
Values may be sent and summed in bfloat16 or wider, within the bound.
No kernel may reach another device: no remote copies, remote signals or barrier semaphores. Data moves between devices by JAX's collectives and lax.ppermute only.
A program may use at most 128 MiB of HBM per device.

v0:
```python
import math
import jax
import jax.numpy as jnp
from jax import lax
from jax.sharding import PartitionSpec as P

NOPE = 64
ROPE_DIM = 32
V_DIM = 64
epsilon = 1e-06
rope_base = 10000.0
masked_value = -1e30


def in_one_piece(arrays, axis, dim, along):
    both = jnp.concatenate(arrays, axis=along)
    out, at, done = (lax.all_gather(both, axis, axis=dim, tiled=True), 0, [])
    for a in arrays:
        done.append(lax.slice_in_dim(out, at, at + a.shape[along], axis=along))
        at += a.shape[along]
    return tuple(done)


def split_up(value, dim, devices):
    before, after = (value.shape[:dim], value.shape[dim + 1 :])
    return jnp.moveaxis(value.reshape(*before, devices, -1, *after), dim, 0)


def sent_and_summed(value, axis, dim):
    devices = lax.axis_size(axis)
    parts = lax.all_to_all(split_up(value, dim, devices), axis, 0, 0, tiled=True)
    return jnp.sum(parts.astype(jnp.float32), axis=0)


def rms_scale(values, gain):
    widened = values.astype(jnp.float32)
    return widened * lax.rsqrt(jnp.mean(widened * widened, axis=-1, keepdims=True) + epsilon) * gain


def tables(positions, rope_width):
    half_width = rope_width // 2
    inverse = rope_base ** (-2.0 * jnp.arange(half_width, dtype=jnp.float32) / rope_width)
    angles = positions.astype(jnp.float32)[:, None] * inverse[None, :]
    return (jnp.cos(angles), jnp.sin(angles))


def rotate(values, cosine, sine):
    half_width = values.shape[-1] // 2
    lower = values[..., :half_width]
    upper = values[..., half_width:]
    return jnp.concatenate([lower * cosine - upper * sine, lower * sine + upper * cosine], axis=-1)


def keep_state(state_in):
    return state_in


def attend_block(running, query_rot, query_pos, key_part, value_part, rope_part):
    amount = key_part.shape[0]
    span_rows = math.gcd(amount, 1024)
    head_count = query_rot.shape[1]
    scale_factor = query_rot.shape[2] ** (-0.5)
    last_query = query_pos[-1]

    def update(state, block_at):
        row_begin = block_at * span_rows
        keys_here = lax.dynamic_slice_in_dim(key_part, row_begin, span_rows, 0).reshape(
            span_rows, head_count, -1
        )
        values_here = lax.dynamic_slice_in_dim(value_part, row_begin, span_rows, 0).reshape(
            span_rows, head_count, -1
        )
        rope_here = lax.dynamic_slice_in_dim(rope_part, row_begin, span_rows, 0)
        key_pos = row_begin + jnp.arange(span_rows, dtype=jnp.int32)

        def advance(state_in):
            top_old, totals, weighted = state_in
            shared = jnp.broadcast_to(
                rope_here[:, None, :], (span_rows, head_count, rope_here.shape[1])
            )
            full_keys = jnp.concatenate([keys_here, shared], axis=-1)
            scores = (
                jnp.einsum("qhd,khd->hqk", query_rot, full_keys, preferred_element_type=jnp.float32)
                * scale_factor
            )
            allowed = key_pos[None, :] <= query_pos[:, None]
            scores = jnp.where(allowed[None], scores, masked_value)
            top_new = jnp.maximum(top_old, jnp.max(scores, axis=-1))
            raised = jnp.where(allowed[None], jnp.exp(scores - top_new[..., None]), 0.0)
            factor = jnp.exp(top_old - top_new)
            totals = totals * factor + jnp.sum(raised, axis=-1)
            weighted = weighted * factor[..., None] + jnp.einsum(
                "hqk,khd->hqd",
                raised.astype(jnp.bfloat16),
                values_here,
                preferred_element_type=jnp.float32,
            )
            return (top_new, totals, weighted)

        return (lax.cond(key_pos[0] <= last_query, advance, keep_state, state), None)

    running, _ = lax.scan(update, running, jnp.arange(amount // span_rows))
    return running


def mixer_half(query, latent, rope_key, latent_gain, key_up, value_up, out_proj):
    query_rows = query.shape[0]
    own_rows = latent.shape[0]
    query_start = lax.axis_index("ep") * query_rows
    key_start = query_start + lax.axis_index("tp") * own_rows
    head_count = query.shape[1] // (NOPE + ROPE_DIM)
    normed = rms_scale(latent, latent_gain).astype(jnp.bfloat16)
    key_cos, key_sin = tables(key_start + jnp.arange(own_rows, dtype=jnp.int32), ROPE_DIM)
    rotated_key = rotate(rope_key.astype(jnp.float32), key_cos, key_sin).astype(jnp.bfloat16)
    query_pos = query_start + jnp.arange(query_rows, dtype=jnp.int32)
    query_cos, query_sin = tables(query_pos, ROPE_DIM)
    query_heads = query.reshape(query_rows, head_count, NOPE + ROPE_DIM)
    turned = rotate(
        query_heads[..., NOPE:].astype(jnp.float32), query_cos[:, None, :], query_sin[:, None, :]
    ).astype(jnp.bfloat16)
    query_rot = jnp.concatenate([query_heads[..., :NOPE], turned], axis=-1)
    last_query = query_start + query_rows - 1
    initial = (
        jnp.full((head_count, query_rows), masked_value, jnp.float32),
        jnp.zeros((head_count, query_rows), jnp.float32),
        jnp.zeros((head_count, query_rows, V_DIM), jnp.float32),
    )
    group_latent, group_rope = in_one_piece((normed, rotated_key), "tp", 0, 1)
    key_part = jnp.dot(group_latent, key_up, preferred_element_type=jnp.float32).astype(
        jnp.bfloat16
    )
    value_part = jnp.dot(group_latent, value_up, preferred_element_type=jnp.float32).astype(
        jnp.bfloat16
    )
    shard_rows = in_one_piece((key_part, value_part, group_rope), "ep", 0, 1)

    def compute(state_in):
        return attend_block(
            state_in, query_rot, query_pos, shard_rows[0], shard_rows[1], shard_rows[2]
        )

    running = lax.cond(jnp.int32(0) <= last_query, compute, keep_state, initial)
    totals = running[1]
    weighted = running[2]
    attention = (
        (weighted / totals[..., None])
        .transpose(1, 0, 2)
        .reshape(query_rows, head_count * V_DIM)
        .astype(jnp.bfloat16)
    )
    own_attention = lax.all_to_all(attention, "tp", split_axis=0, concat_axis=1, tiled=True)
    return jnp.dot(own_attention, out_proj, preferred_element_type=jnp.float32).astype(jnp.bfloat16)


def expert_half(tokens, moe_gain, routes, group_prob, expert_prob, w_gate, w_up, w_down):
    row_count, model_width = tokens.shape
    top_count = routes.shape[1]
    expert_count = lax.axis_size("ep")
    capacity = 2 * top_count * row_count // expert_count
    normed = rms_scale(tokens, moe_gain).astype(jnp.bfloat16)
    flat_routes = routes.reshape(-1)
    onehot = (flat_routes[:, None] == jnp.arange(expert_count, dtype=jnp.int32)[None, :]).astype(
        jnp.int32
    )
    earlier = jnp.cumsum(onehot, axis=0) - onehot
    slot_index = jnp.sum(earlier * onehot, axis=1)
    target = flat_routes * capacity + slot_index
    owner = target[None, :] == jnp.arange(expert_count * capacity, dtype=jnp.int32)[:, None]
    dispatch_table = jnp.any(
        owner.reshape(expert_count * capacity, row_count, top_count), axis=2
    ).astype(jnp.bfloat16)
    outgoing = jnp.dot(dispatch_table, normed, preferred_element_type=jnp.float32).astype(
        jnp.bfloat16
    )
    outgoing = outgoing.reshape(expert_count, capacity, model_width)
    arrived = lax.all_to_all(outgoing, "ep", split_axis=0, concat_axis=0, tiled=True)
    sources, slots, _ = arrived.shape
    flat_rows = arrived.reshape(sources * slots, model_width)
    shard_rows = lax.all_gather(flat_rows, "tp", axis=0, tiled=True)
    gate_values = jnp.dot(shard_rows, w_gate[0], preferred_element_type=jnp.float32)
    up_values = jnp.dot(shard_rows, w_up[0], preferred_element_type=jnp.float32)
    hidden = (jax.nn.silu(gate_values) * up_values).astype(jnp.bfloat16)

    def lower(offset, amount):
        return jnp.dot(hidden, w_down[0], preferred_element_type=jnp.float32)

    summed = sent_and_summed(
        lower(jnp.int32(0), sources * slots * lax.axis_size("tp")).astype(jnp.bfloat16), "tp", 0
    )
    result = summed.astype(jnp.bfloat16).reshape(sources, slots, model_width)
    returned = lax.all_to_all(result, "ep", split_axis=0, concat_axis=0, tiled=True)
    returned_flat = returned.reshape(expert_count * capacity, model_width)
    picked = returned_flat[target].reshape(row_count, top_count, model_width).astype(jnp.float32)
    shares = group_prob[:, None] * expert_prob / jnp.sum(expert_prob, axis=1, keepdims=True)
    return jnp.sum(shares[:, :, None] * picked, axis=1).astype(jnp.bfloat16)


def body(
    query,
    latent,
    rope_key,
    latent_gain,
    key_up,
    value_up,
    out_proj,
    tokens,
    moe_gain,
    routes,
    group_prob,
    expert_prob,
    w_gate,
    w_up,
    w_down,
):
    mixed = mixer_half(query, latent, rope_key, latent_gain, key_up, value_up, out_proj)
    moe_out = expert_half(tokens, moe_gain, routes, group_prob, expert_prob, w_gate, w_up, w_down)
    return (mixed, moe_out)


def solution(mesh):
    return jax.shard_map(
        body,
        mesh=mesh,
        in_specs=(
            P("ep", "tp"),
            P(("ep", "tp"), None),
            P(("ep", "tp"), None),
            P(),
            P(None, "tp"),
            P(None, "tp"),
            P(),
            P(("ep", "tp"), None),
            P(),
            P(("ep", "tp"), None),
            P(("ep", "tp")),
            P(("ep", "tp"), None),
            P("ep", None, "tp"),
            P("ep", None, "tp"),
            P("ep", "tp", None),
        ),
        out_specs=(P(("ep", "tp"), None), P(("ep", "tp"), None)),
        check_vma=False,
    )
```

profile of v0, /device:TPU:224, one launch (start us, length us, event | category | flops | bytes accessed | tf_op | source)
XLA Modules:
  0.0 333.0 jit_solution(12804921602035847933)
XLA Ops:
  7.2 0.8 copy.49
  9.0 1.1 fusion.27
  10.1 1.5 convolution_convert_fusion.1
  12.0 36.0 %all_to_all.31 = bf16[64,4,2048]{2,1,0:T(4,128)(2,1)S(1)} all-to-all(bf16[64,4,2048]{2,1,0:T(4,128)(2,1)S(1)} %reshape.209), channel_id=1, replica_groups=mesh['ep'=64,'tp'=4] {'ep'}, dimensions={0} | all-to-all | bytes 2097152 | tf_op jit(solution)/shard_map/all_to_all | solution.py:176
  48.1 1.1 reshape.210
  50.0 12.4 %all_gather.9 = bf16[128,544]{1,0:T(8,128)(2,1)S(1)} all-gather(bf16[32,544]{1,0:T(8,128)(2,1)S(1)} %pad_maximum_fusion.2), channel_id=1, replica_groups=mesh['ep'=64,'tp'=4] {'tp'}, dimensions={0}, use_global_device_ids=true | all-gather | bytes 174080 | tf_op jit(solution)/shard_map/all_gather | solution.py:17
  62.8 0.7 pad_maximum_fusion
  63.6 35.2 %all-gather.5.cloned.1.call-done = bf16[1024,2048]{1,0:T(8,128)(2,1)} async-done(((bf16[256,2048]{1,0:T(8,128)(2,1)}), bf16[1024,2048]{1,0:T(8,128)(2,1)}) %all-gather.5.cloned.1.call-update) | async-done | bytes 4194320 | tf_op jit(solution)/shard_map/all_gather | solution.py:179
  98.8 4.4 %fusion.20 = f32[1024,256]{1,0:T(8,128)} fusion(bf16[1024,2048]{1,0:T(8,128)(2,1)} %all-gather.5.cloned.1.call-done, bf16[1,2048,256]{2,1,0:T(8,128)(2,1)S(1)} %copy-done.9), kind=kOutput, calls=%fused_computation.36 | convolution fusion | flops 1073741824 | bytes 6291456 | tf_op jit(solution)/shard_map/dot_general | solution.py:180
  103.2 8.8 %convolution_convert_fusion = bf16[1024,2048]{1,0:T(8,128)(2,1)} fusion(bf16[1024,2048]{1,0:T(8,128)(2,1)} %all-gather.5.cloned.1.call-done, bf16[1,256,2048]{2,1,0:T(8,128)(2,1)S(1)} %copy-done, bf16[1,2048,256]{2,1,0:T(8,128)(2,1)S(1)} %copy-done.10, f32[1024,256]{1,0:T(8,128)} %fusion.20), kind=kOutput, calls=%fused_computation.27 | convolution fusion | flops 2151153664 | bytes 11534336 | tf_op jit(solution)/shard_map/dot_general | solution.py:185
  112.0 54.6 %all_to_all.32 = bf16[4,256,2048]{2,1,0:T(8,128)(2,1)} all-to-all(bf16[4,256,2048]{2,1,0:T(8,128)(2,1)} %bitcast.54), channel_id=1, replica_groups=mesh['ep'=64,'tp'=4] {'tp'}, dimensions={0} | all-to-all | bytes 8388608 | tf_op jit(solution)/shard_map/all_to_all | solution.py:31
  166.6 3.4 %reduce_sum.78 = bf16[256,2048]{1,0:T(8,128)(2,1)S(1)} reduce(bf16[4,256,2048]{2,1,0:T(8,128)(2,1)} %all_to_all.32, bf16[]{:T(256)} %constant.106.clone.1), dimensions={0}, to_apply=%region_14.15 | reduce | flops 1572864 | bytes 5242882 | tf_op jit(solution)/shard_map/reduce_sum | solution.py:32
  170.1 1.2 reshape.212
  171.3 10.0 %all-to-all-start.3 = ((bf16[64,4,2048]{2,1,0:T(4,128)(2,1)}), bf16[64,4,2048]{2,1,0:T(4,128)(2,1)S(1)}, u32[]{:S(2)}, u32[]{:S(2)}) async-start(bf16[64,4,2048]{2,1,0:T(4,128)(2,1)} %reshape.212), calls=%async_computation.3 | async-start | bytes 2097152 | tf_op jit(solution)/shard_map/all_to_all | solution.py:191
  181.9 26.5 %all-to-all-done.3 = bf16[64,4,2048]{2,1,0:T(4,128)(2,1)S(1)} async-done(((bf16[64,4,2048]{2,1,0:T(4,128)(2,1)}), bf16[64,4,2048]{2,1,0:T(4,128)(2,1)S(1)}, u32[]{:S(2)}, u32[]{:S(2)}) %all-to-all-start.3) | async-done | bytes 1048608 | tf_op jit(solution)/shard_map/all_to_all | solution.py:191
  208.7 0.9 gather_fusion
  209.7 0.7 reshape.214
  210.4 101.0 %conditional.2 = (f32[4,128]{1,0:T(4,128)}, f32[4,128,64]{1,2,0:T(8,128)}) conditional(s32[]{:T(128)} %convert_element_type.89, () %tuple.36, (bf16[8192,544]{1,0:T(8,128)(2,1)}, s32[]{:T(128)}, s32[128]{0:T(128)S(1)}, bf16[128,4,96]{0,2,1:T(8,128)(2,1)S(1)}) %tuple.37), branch_computations={%region_1.0_spmd, %region_2.9_spmd} | conditional | flops 176359552 | bytes 46872600 | solution.py:142
  210.4 12.9 %copy.45 = bf16[8192,544]{0,1:T(8,128)(2,1)} copy(bf16[8192,544]{1,0:T(8,128)(2,1)} %get-tuple-element.221) | data formatting | bytes 17825792 | tf_op jit(solution)/shard_map
  223.3 6.1 %fusion.53 = (bf16[8192,256]{0,1:T(8,128)(2,1)}, bf16[8192,256]{0,1:T(8,128)(2,1)}) fusion(bf16[8192,544]{0,1:T(8,128)(2,1)} %copy.45), kind=kLoop, calls=%fused_computation.97 | loop fusion | bytes 16777216 | tf_op jit(solution)/shard_map/slice | solution.py:19
  229.4 1.1 slice.53
  231.1 0.7 broadcast_in_dim.75
  232.3 79.0 %while.13 = (s32[]{:T(128)}, f32[4,128]{1,0:T(4,128)S(1)}, f32[4,128]{1,0:T(4,128)}, f32[4,128,64]{1,2,0:T(8,128)}, s32[8]{0:T(128)S(1)}, /*index=5*/s32[]{:T(12...) while((s32[]{:T(128)}, f32[4,128]{1,0:T(4,128)S(1)}, ...), condition=%wide.region_8.8_spmd, body=%wide.region_3.7_spmd.sunk | while | flops 176359424 | bytes 11084641 | solution.py:102
  235.2 7.0 %conditional.4 = ((f32[4,128]{1,0:T(4,128)S(1)}, f32[4,128]{1,0:T(4,128)}, f32[4,128,64]{1,2,0:T(8,128)})) conditional(s32[]{:T(128)} %convert_element_type.152, (f32[4,128]{1,0:T(4,128)S(1)}, f32[4,128]{1,0:T(4,128)}, f32[4,128,64]{1,2,0:T(8,128)}) %tuple.61, (s32[1024]{0:T(1024)S(1)}, s32[128]{0:T(128)S(1)}, s32[]{:T(128)}, ...), branch_computations={%region_4.3_spmd, %region_5.6_spmd} | conditional | flops 176358400 | bytes 11080266 | solution.py:100
  235.2 1.9 constant_dynamic-slice_fusion
  238.6 1.3 multiply_add_fusion
  239.9 2.3 convolution_add_fusion
  245.1 7.0 %conditional.4 = ((f32[4,128]{1,0:T(4,128)S(1)}, f32[4,128]{1,0:T(4,128)}, f32[4,128,64]{1,2,0:T(8,128)})) conditional(s32[]{:T(128)} %convert_element_type.152, (f32[4,128]{1,0:T(4,128)S(1)}, f32[4,128]{1,0:T(4,128)}, f32[4,128,64]{1,2,0:T(8,128)}) %tuple.61, (s32[1024]{0:T(1024)S(1)}, s32[128]{0:T(128)S(1)}, s32[]{:T(128)}, ...), branch_computations={%region_4.3_spmd, %region_5.6_spmd} | conditional | flops 176358400 | bytes 11080266 | solution.py:100
  245.1 1.9 constant_dynamic-slice_fusion
  247.3 0.6 fusion
  248.5 1.3 multiply_add_fusion
  249.8 2.3 convolution_add_fusion
  255.0 7.0 %conditional.4 = ((f32[4,128]{1,0:T(4,128)S(1)}, f32[4,128]{1,0:T(4,128)}, f32[4,128,64]{1,2,0:T(8,128)})) conditional(s32[]{:T(128)} %convert_element_type.152, (f32[4,128]{1,0:T(4,128)S(1)}, f32[4,128]{1,0:T(4,128)}, f32[4,128,64]{1,2,0:T(8,128)}) %tuple.61, (s32[1024]{0:T(1024)S(1)}, s32[128]{0:T(128)S(1)}, s32[]{:T(128)}, ...), branch_computations={%region_4.3_spmd, %region_5.6_spmd} | conditional | flops 176358400 | bytes 11080266 | solution.py:100
  255.0 1.9 constant_dynamic-slice_fusion
  258.4 1.3 multiply_add_fusion
  259.7 2.3 convolution_add_fusion
  264.9 7.0 %conditional.4 = ((f32[4,128]{1,0:T(4,128)S(1)}, f32[4,128]{1,0:T(4,128)}, f32[4,128,64]{1,2,0:T(8,128)})) conditional(s32[]{:T(128)} %convert_element_type.152, (f32[4,128]{1,0:T(4,128)S(1)}, f32[4,128]{1,0:T(4,128)}, f32[4,128,64]{1,2,0:T(8,128)}) %tuple.61, (s32[1024]{0:T(1024)S(1)}, s32[128]{0:T(128)S(1)}, s32[]{:T(128)}, ...), branch_computations={%region_4.3_spmd, %region_5.6_spmd} | conditional | flops 176358400 | bytes 11080266 | solution.py:100
  264.9 1.9 constant_dynamic-slice_fusion
  267.1 0.6 fusion
  268.3 1.3 multiply_add_fusion
  269.6 2.3 convolution_add_fusion
  274.8 7.0 %conditional.4 = ((f32[4,128]{1,0:T(4,128)S(1)}, f32[4,128]{1,0:T(4,128)}, f32[4,128,64]{1,2,0:T(8,128)})) conditional(s32[]{:T(128)} %convert_element_type.152, (f32[4,128]{1,0:T(4,128)S(1)}, f32[4,128]{1,0:T(4,128)}, f32[4,128,64]{1,2,0:T(8,128)}) %tuple.61, (s32[1024]{0:T(1024)S(1)}, s32[128]{0:T(128)S(1)}, s32[]{:T(128)}, ...), branch_computations={%region_4.3_spmd, %region_5.6_spmd} | conditional | flops 176358400 | bytes 11080266 | solution.py:100
  274.8 1.9 constant_dynamic-slice_fusion
  278.2 1.3 multiply_add_fusion
  279.4 2.3 convolution_add_fusion
  284.6 7.0 %conditional.4 = ((f32[4,128]{1,0:T(4,128)S(1)}, f32[4,128]{1,0:T(4,128)}, f32[4,128,64]{1,2,0:T(8,128)})) conditional(s32[]{:T(128)} %convert_element_type.152, (f32[4,128]{1,0:T(4,128)S(1)}, f32[4,128]{1,0:T(4,128)}, f32[4,128,64]{1,2,0:T(8,128)}) %tuple.61, (s32[1024]{0:T(1024)S(1)}, s32[128]{0:T(128)S(1)}, s32[]{:T(128)}, ...), branch_computations={%region_4.3_spmd, %region_5.6_spmd} | conditional | flops 176358400 | bytes 11080266 | solution.py:100
  284.7 1.9 constant_dynamic-slice_fusion
  286.9 0.6 fusion
  288.1 1.3 multiply_add_fusion
  289.3 2.3 convolution_add_fusion
  294.5 7.0 %conditional.4 = ((f32[4,128]{1,0:T(4,128)S(1)}, f32[4,128]{1,0:T(4,128)}, f32[4,128,64]{1,2,0:T(8,128)})) conditional(s32[]{:T(128)} %convert_element_type.152, (f32[4,128]{1,0:T(4,128)S(1)}, f32[4,128]{1,0:T(4,128)}, f32[4,128,64]{1,2,0:T(8,128)}) %tuple.61, (s32[1024]{0:T(1024)S(1)}, s32[128]{0:T(128)S(1)}, s32[]{:T(128)}, ...), branch_computations={%region_4.3_spmd, %region_5.6_spmd} | conditional | flops 176358400 | bytes 11080266 | solution.py:100
  294.5 1.9 constant_dynamic-slice_fusion
  297.9 1.3 multiply_add_fusion
  299.2 2.3 convolution_add_fusion
  304.4 6.9 %conditional.4 = ((f32[4,128]{1,0:T(4,128)S(1)}, f32[4,128]{1,0:T(4,128)}, f32[4,128,64]{1,2,0:T(8,128)})) conditional(s32[]{:T(128)} %convert_element_type.152, (f32[4,128]{1,0:T(4,128)S(1)}, f32[4,128]{1,0:T(4,128)}, f32[4,128,64]{1,2,0:T(8,128)}) %tuple.61, (s32[1024]{0:T(1024)S(1)}, s32[128]{0:T(128)S(1)}, s32[]{:T(128)}, ...), branch_computations={%region_4.3_spmd, %region_5.6_spmd} | conditional | flops 176358400 | bytes 11080266 | solution.py:100
  304.4 1.8 constant_dynamic-slice_fusion
  307.8 1.3 multiply_add_fusion
  309.1 2.3 convolution_add_fusion
  311.3 0.9 fusion.41
  312.4 0.8 convert_element_type.100
  313.2 3.7 %all-to-all-start = ((bf16[4,32,256]{2,1,0:T(8,128)(2,1)}), bf16[4,32,256]{2,1,0:T(8,128)(2,1)S(1)}, u32[]{:S(2)}, u32[]{:S(2)}) async-start(bf16[4,32,256]{2,1,0:T(8,128)(2,1)} %convert_element_type.100), calls=%async_computation | async-start | bytes 131072 | tf_op jit(solution)/shard_map/all_to_all | solution.py:151
  316.9 2.2 multiply_reduce_fusion
  319.1 3.4 %all-to-all-done = bf16[4,32,256]{2,1,0:T(8,128)(2,1)S(1)} async-done(((bf16[4,32,256]{2,1,0:T(8,128)(2,1)}), bf16[4,32,256]{2,1,0:T(8,128)(2,1)S(1)}, u32[]{:S(2)}, u32[]{:S(2)}) %all-to-all-start) | async-done | bytes 65568 | tf_op jit(solution)/shard_map/all_to_all | solution.py:151
  322.5 3.7 %convolution_convert_fusion.2 = bf16[32,2048]{1,0:T(8,128)(2,1)} fusion(bf16[32,1024]{1,0:T(8,128)(2,1)S(1)} %bitcast.57, bf16[1024,2048]{1,0:T(8,128)(2,1)} %param.27), kind=kOutput, calls=%fused_computation.29 | convolution fusion | flops 134283264 | bytes 4390912 | tf_op jit(solution)/shard_map/dot_general | solution.py:152
  (150 shorter events, 23.5 us)
Async XLA Ops:
  7.2 96.0 %copy-start = (bf16[1,256,2048]{2,1,0:T(8,128)(2,1)S(1)}, bf16[1,256,2048]{2,1,0:T(8,128)(2,1)}, u32[]{:S(2)}) copy-start(bf16[1,256,2048]{2,1,0:T(8,128)(2,1)} %param.35) | copy-start | bytes 3145732
  7.2 91.6 %all-gather.5.cloned.1.call-start = ((), (), s32[]{:S(2)}) async-start(), calls=%async_computation.5 | async-start | bytes 5242880 | tf_op jit(solution)/shard_map/all_gather | solution.py:179
  48.0 1.3 copy-start.5
  48.0 1.7 copy-start.3
  48.0 1.8 copy-start.7
  48.1 14.4 %copy-start.1 = (bf16[512,256]{1,0:T(8,128)(2,1)S(1)}, bf16[512,256]{1,0:T(8,128)(2,1)}, u32[]{:S(2)}) copy-start(bf16[512,256]{1,0:T(8,128)(2,1)} %param.26) | copy-start | bytes 786436
  48.1 14.6 %copy-start.2 = (bf16[512,256]{1,0:T(8,128)(2,1)S(1)}, bf16[512,256]{1,0:T(8,128)(2,1)}, u32[]{:S(2)}) copy-start(bf16[512,256]{1,0:T(8,128)(2,1)} %param.25) | copy-start | bytes 786436
  49.2 49.6 %copy-start.9 = (bf16[1,2048,256]{2,1,0:T(8,128)(2,1)S(1)}, bf16[1,2048,256]{2,1,0:T(8,128)(2,1)}, u32[]{:S(2)}) copy-start(bf16[1,2048,256]{2,1,0:T(8,128)(2,1)} %param.33) | copy-start | bytes 3145732
  49.2 161.1 %all-gather.3.cloned.1.call-start = ((), (), s32[]{:S(2)}) async-start(), calls=%async_computation.4 | async-start | bytes 10649600 | tf_op jit(solution)/shard_map/all_gather | solution.py:17
  63.5 39.7 %copy-start.10 = (bf16[1,2048,256]{2,1,0:T(8,128)(2,1)S(1)}, bf16[1,2048,256]{2,1,0:T(8,128)(2,1)}, u32[]{:S(2)}) copy-start(bf16[1,2048,256]{2,1,0:T(8,128)(2,1)} %param.34) | copy-start | bytes 3145732
  170.0 11.3 %copy-start.4 = (bf16[128,384]{1,0:T(8,128)(2,1)S(1)}, bf16[128,384]{1,0:T(8,128)(2,1)}, u32[]{:S(2)}) copy-start(bf16[128,384]{1,0:T(8,128)(2,1)} %param.21) | copy-start | bytes 294916
  170.0 11.6 %copy-start.6 = (f32[64,2]{0,1:T(2,128)S(1)}, f32[64,2]{0,1:T(2,128)}, u32[]{:S(2)}) copy-start(f32[64,2]{0,1:T(2,128)} %param.32) | copy-start | bytes 1540
  170.0 11.6 %copy-start.8 = (f32[64]{0:T(128)S(1)}, f32[64]{0:T(128)}, u32[]{:S(2)}) copy-start(f32[64]{0:T(128)} %param.31) | copy-start | bytes 772
  171.3 37.2 %all-to-all-start.3 = ((bf16[64,4,2048]{2,1,0:T(4,128)(2,1)}), bf16[64,4,2048]{2,1,0:T(4,128)(2,1)S(1)}, u32[]{:S(2)}, u32[]{:S(2)}) async-start(bf16[64,4,2048]{2,1,0:T(4,128)(2,1)} %reshape.212), calls=%async_computation.3 | async-start | bytes 2097152 | tf_op jit(solution)/shard_map/all_to_all | solution.py:191
  313.2 9.3 %all-to-all-start = ((bf16[4,32,256]{2,1,0:T(8,128)(2,1)}), bf16[4,32,256]{2,1,0:T(8,128)(2,1)S(1)}, u32[]{:S(2)}, u32[]{:S(2)}) async-start(bf16[4,32,256]{2,1,0:T(8,128)(2,1)} %convert_element_type.100), calls=%async_computation | async-start | bytes 131072 | tf_op jit(solution)/shard_map/all_to_all | solution.py:151
Sparse Core Ops, SparseCore 0:
  49.4 49.3 all-gather.4
  102.1 91.5 all-gather.2
where the time goes:
time: 335 us; the launch traced here: 333 us
  blocking collectives  103 us (31%)
  waiting for transfers between devices  65.2 us (19%)
  local copies, waits for them, and re-layouts  54 us (16%)
  matrix products  42 us (13%)
  other arithmetic  25.7 us (8%)
  loops' own time  15 us (4%)
  between operations  14.4 us (4%)
  starting transfers between devices  13.8 us (4%)
    all_to_all x1, blocking collectives, sent_and_summed(): lax.all_to_all(split_up(value, dim, devices), axis, 0, 0, tiled=True)  54.6 us
    all_to_all x1, blocking collectives, expert_half(): lax.all_to_all(outgoing, 'ep', split_axis=0, concat_axis=0, tiled=True)  36 us
    all_gather x1, waiting for transfers between devices, expert_half(): shard_rows = lax.all_gather(flat_rows, 'tp', axis=0, tiled=True)  35.2 us
    all_to_all x1, waiting for transfers between devices, expert_half(): lax.all_to_all(result, 'ep', split_axis=0, concat_axis=0, tiled=True)  26.5 us
    dot_general x8, matrix products, advance(): jnp.einsum('hqk,khd->hqd', raised.astype(jnp.bfloat16), values_here, pref...  18.2 us
    dynamic_slice x8, local copies, waits for them, and re-layouts, update(): lax.dynamic_slice_in_dim(value_part, row_begin, span_rows, 0)  15 us
    another operation x1, loops' own time, attend_block(): running, _ = lax.scan(update, running, jnp.arange(amount // span_rows))  14.5 us
    another operation x3, local copies, waits for them, and re-layouts  13.1 us
  transfers between devices with their start and end apart: 4, of which 3 were waited for; matrix products, arithmetic and copies ran while one was open for 7% of the time, Pallas kernels for 0%

commit v1 on v0

--- a/solution.py
+++ b/solution.py
@@ -176,7 +176,9 @@
     arrived = lax.all_to_all(outgoing, "ep", split_axis=0, concat_axis=0, tiled=True)
     sources, slots, _ = arrived.shape
     flat_rows = arrived.reshape(sources * slots, model_width)
-    shard_rows = lax.all_gather(flat_rows, "tp", axis=0, tiled=True)
+    shard_rows = jnp.concatenate(
+        lax.all_to_all(jnp.stack([flat_rows] * lax.axis_size("tp")), "tp", 0, 0), axis=0
+    )
     gate_values = jnp.dot(shard_rows, w_gate[0], preferred_element_type=jnp.float32)
     up_values = jnp.dot(shard_rows, w_up[0], preferred_element_type=jnp.float32)
     hidden = (jax.nn.silu(gate_values) * up_values).astype(jnp.bfloat16)

time: 335 us -> 356 us (1.063)
  blocking collectives: 103 us -> 162 us
  waiting for transfers between devices: 65.2 us -> 29.7 us
  starting transfers between devices: 13.8 us -> 9.91 us
    all_to_all x0 -> x1, blocking collectives: none -> 52.8 us  [expert_half(): lax.all_to_all(jnp.stack([flat_rows] * lax.axis_size('tp')), 'tp', 0, 0)]
    all_gather x1 -> x0, waiting for transfers between devices: 35.2 us -> none  [expert_half(): shard_rows = lax.all_gather(flat_rows, 'tp', axis=0, tiled=True)]
    all_to_all x1, blocking collectives: 36 us -> 42.4 us  [expert_half(): lax.all_to_all(outgoing, 'ep', split_axis=0, concat_axis=0, tiled=True)]
    another operation x3 -> x5, local copies, waits for them, and re-layouts: 13.1 us -> 14.9 us
  transfers between devices with their start and end apart: 4 -> 3, of which waited for: 3 -> 2; matrix products, arithmetic and copies ran while one was open for 7% -> 7% of each run, Pallas kernels for 0% -> 0%
where the time goes in v1:
time: 356 us; the launch traced here: 354 us
  blocking collectives  162 us (46%)
  local copies, waits for them, and re-layouts  57.5 us (16%)
  matrix products  39.4 us (11%)
  waiting for transfers between devices  29.7 us (8%)
  other arithmetic  25.9 us (7%)
  loops' own time  15.4 us (4%)
  between operations  14.4 us (4%)
  starting transfers between devices  9.91 us (3%)
    all_to_all x1, blocking collectives, sent_and_summed(): lax.all_to_all(split_up(value, dim, devices), axis, 0, 0, tiled=True)  54.1 us
    all_to_all x1, blocking collectives, expert_half(): lax.all_to_all(jnp.stack([flat_rows] * lax.axis_size('tp')), 'tp', 0, 0)  52.8 us
    all_to_all x1, blocking collectives, expert_half(): lax.all_to_all(outgoing, 'ep', split_axis=0, concat_axis=0, tiled=True)  42.4 us
    all_to_all x1, waiting for transfers between devices, expert_half(): lax.all_to_all(result, 'ep', split_axis=0, concat_axis=0, tiled=True)  26.3 us
    dot_general x8, matrix products, advance(): jnp.einsum('hqk,khd->hqd', raised.astype(jnp.bfloat16), values_here, pref...  18 us
    dynamic_slice x8, local copies, waits for them, and re-layouts, update(): lax.dynamic_slice_in_dim(value_part, row_begin, span_rows, 0)  14.9 us
    another operation x1, loops' own time, attend_block(): running, _ = lax.scan(update, running, jnp.arange(amount // span_rows))  14.9 us
    another operation x3, local copies, waits for them, and re-layouts  13.1 us
  transfers between devices with their start and end apart: 3, of which 2 were waited for; matrix products, arithmetic and copies ran while one was open for 7% of the time, Pallas kernels for 0%

profile of v1, /device:TPU:224, one launch (start us, length us, event | category | flops | bytes accessed | tf_op | source)
XLA Modules:
  0.0 353.9 jit_solution(7917138097720309819)
XLA Ops:
  7.3 0.9 copy.41
  8.5 0.9 fusion.37
  9.3 0.8 fusion.39
  10.3 12.4 %all_gather.6 = bf16[128,544]{1,0:T(8,128)(2,1)S(1)} all-gather(bf16[32,544]{1,0:T(8,128)(2,1)S(1)} %pad_maximum_fusion.2), channel_id=1, replica_groups=mesh['ep'=64,'tp'=4] {'tp'}, dimensions={0}, use_global_device_ids=true | all-gather | bytes 174080 | tf_op jit(solution)/shard_map/all_gather | solution.py:17
  22.7 1.1 convolution_convert_fusion.3
  23.8 1.1 convolution_convert_fusion.4
  25.0 0.7 pad_maximum_fusion
  25.7 0.8 copy.49
  28.5 42.4 %all_to_all.36 = bf16[64,4,2048]{2,1,0:T(4,128)(2,1)} all-to-all(bf16[64,4,2048]{2,1,0:T(4,128)(2,1)S(1)} %reshape.211), channel_id=1, replica_groups=mesh['ep'=64,'tp'=4] {'ep'}, dimensions={0} | all-to-all | bytes 2097152 | tf_op jit(solution)/shard_map/all_to_all | solution.py:176
  70.9 1.3 stack_reshape.2
  72.8 52.8 %all_to_all.37 = bf16[4,256,2048]{2,1,0:T(8,128)(2,1)S(1)} all-to-all(bf16[4,256,2048]{2,1,0:T(8,128)(2,1)S(1)} %stack.3), channel_id=1, replica_groups=mesh['ep'=64,'tp'=4] {'tp'}, dimensions={0} | all-to-all | bytes 8388608 | tf_op jit(solution)/shard_map/all_to_all | solution.py:180
  125.6 2.0 copy-done.2
  127.5 1.3 fusion.20
  128.8 8.6 %convolution_convert_fusion = bf16[1024,2048]{1,0:T(8,128)(2,1)} fusion(bf16[1024,2048]{1,0:T(8,128)(2,1)} %bitcast.56, bf16[1,256,2048]{2,1,0:T(8,128)(2,1)S(1)} %copy-done, bf16[1,2048,256]{2,1,0:T(8,128)(2,1)S(1)} %copy-done.9, f32[1024,256]{1,0:T(8,128)S(1)} %fusion.20), kind=kOutput, calls=%fused_computation.27 | convolution fusion | flops 2151153664 | bytes 11534336 | tf_op jit(solution)/shard_map/dot_general | solution.py:187
  137.4 54.1 %all_to_all.38 = bf16[4,256,2048]{2,1,0:T(8,128)(2,1)} all-to-all(bf16[4,256,2048]{2,1,0:T(8,128)(2,1)} %bitcast.57), channel_id=1, replica_groups=mesh['ep'=64,'tp'=4] {'tp'}, dimensions={0} | all-to-all | bytes 8388608 | tf_op jit(solution)/shard_map/all_to_all | solution.py:31
  191.5 3.1 reduce_sum.78
  194.6 1.2 reshape.214
  195.8 6.6 %all-to-all-start.4 = ((bf16[64,4,2048]{2,1,0:T(4,128)(2,1)}), bf16[64,4,2048]{2,1,0:T(4,128)(2,1)S(1)}, u32[]{:S(2)}, u32[]{:S(2)}) async-start(bf16[64,4,2048]{2,1,0:T(4,128)(2,1)} %reshape.214), calls=%async_computation.4 | async-start | bytes 2097152 | tf_op jit(solution)/shard_map/all_to_all | solution.py:193
  203.1 26.3 %all-to-all-done.4 = bf16[64,4,2048]{2,1,0:T(4,128)(2,1)S(1)} async-done(((bf16[64,4,2048]{2,1,0:T(4,128)(2,1)}), bf16[64,4,2048]{2,1,0:T(4,128)(2,1)S(1)}, u32[]{:S(2)}, u32[]{:S(2)}) %all-to-all-start.4) | async-done | bytes 1048608 | tf_op jit(solution)/shard_map/all_to_all | solution.py:193
  229.6 0.9 gather_fusion
  231.3 101.3 %conditional.2 = (f32[4,128]{1,0:T(4,128)}, f32[4,128,64]{1,2,0:T(8,128)}) conditional(s32[]{:T(128)} %convert_element_type.89, () %tuple.36, (bf16[8192,544]{1,0:T(8,128)(2,1)}, s32[]{:T(128)}, s32[128]{0:T(128)S(1)}, bf16[128,4,96]{0,2,1:T(8,128)(2,1)S(1)}) %tuple.37), branch_computations={%region_1.0_spmd, %region_2.9_spmd} | conditional | flops 176359552 | bytes 46872600 | solution.py:142
  231.3 12.9 %copy.45 = bf16[8192,544]{0,1:T(8,128)(2,1)} copy(bf16[8192,544]{1,0:T(8,128)(2,1)} %get-tuple-element.221) | data formatting | bytes 17825792 | tf_op jit(solution)/shard_map
  244.2 6.0 %fusion.53 = (bf16[8192,256]{0,1:T(8,128)(2,1)}, bf16[8192,256]{0,1:T(8,128)(2,1)}) fusion(bf16[8192,544]{0,1:T(8,128)(2,1)} %copy.45), kind=kLoop, calls=%fused_computation.97 | loop fusion | bytes 16777216 | tf_op jit(solution)/shard_map/slice | solution.py:19
  250.2 1.1 slice.53
  252.0 0.7 broadcast_in_dim.75
  253.2 79.3 %while.13 = (s32[]{:T(128)}, f32[4,128]{1,0:T(4,128)S(1)}, f32[4,128]{1,0:T(4,128)}, f32[4,128,64]{1,2,0:T(8,128)}, s32[8]{0:T(128)S(1)}, /*index=5*/s32[]{:T(12...) while((s32[]{:T(128)}, f32[4,128]{1,0:T(4,128)S(1)}, ...), condition=%wide.region_8.8_spmd, body=%wide.region_3.7_spmd.sunk | while | flops 176359424 | bytes 11084641 | solution.py:102
  256.2 6.9 %conditional.4 = ((f32[4,128]{1,0:T(4,128)S(1)}, f32[4,128]{1,0:T(4,128)}, f32[4,128,64]{1,2,0:T(8,128)})) conditional(s32[]{:T(128)} %convert_element_type.152, (f32[4,128]{1,0:T(4,128)S(1)}, f32[4,128]{1,0:T(4,128)}, f32[4,128,64]{1,2,0:T(8,128)}) %tuple.61, (s32[1024]{0:T(1024)S(1)}, s32[128]{0:T(128)S(1)}, s32[]{:T(128)}, ...), branch_computations={%region_4.3_spmd, %region_5.6_spmd} | conditional | flops 176358400 | bytes 11080266 | solution.py:100
  256.2 1.9 constant_dynamic-slice_fusion
  259.6 1.3 multiply_add_fusion
  260.9 2.2 convolution_add_fusion
  266.1 6.9 %conditional.4 = ((f32[4,128]{1,0:T(4,128)S(1)}, f32[4,128]{1,0:T(4,128)}, f32[4,128,64]{1,2,0:T(8,128)})) conditional(s32[]{:T(128)} %convert_element_type.152, (f32[4,128]{1,0:T(4,128)S(1)}, f32[4,128]{1,0:T(4,128)}, f32[4,128,64]{1,2,0:T(8,128)}) %tuple.61, (s32[1024]{0:T(1024)S(1)}, s32[128]{0:T(128)S(1)}, s32[]{:T(128)}, ...), branch_computations={%region_4.3_spmd, %region_5.6_spmd} | conditional | flops 176358400 | bytes 11080266 | solution.py:100
  266.1 1.9 constant_dynamic-slice_fusion
  269.5 1.3 multiply_add_fusion
  270.8 2.2 convolution_add_fusion
  276.0 6.9 %conditional.4 = ((f32[4,128]{1,0:T(4,128)S(1)}, f32[4,128]{1,0:T(4,128)}, f32[4,128,64]{1,2,0:T(8,128)})) conditional(s32[]{:T(128)} %convert_element_type.152, (f32[4,128]{1,0:T(4,128)S(1)}, f32[4,128]{1,0:T(4,128)}, f32[4,128,64]{1,2,0:T(8,128)}) %tuple.61, (s32[1024]{0:T(1024)S(1)}, s32[128]{0:T(128)S(1)}, s32[]{:T(128)}, ...), branch_computations={%region_4.3_spmd, %region_5.6_spmd} | conditional | flops 176358400 | bytes 11080266 | solution.py:100
  276.1 1.9 constant_dynamic-slice_fusion
  279.5 1.3 multiply_add_fusion
  280.7 2.2 convolution_add_fusion
  286.0 6.9 %conditional.4 = ((f32[4,128]{1,0:T(4,128)S(1)}, f32[4,128]{1,0:T(4,128)}, f32[4,128,64]{1,2,0:T(8,128)})) conditional(s32[]{:T(128)} %convert_element_type.152, (f32[4,128]{1,0:T(4,128)S(1)}, f32[4,128]{1,0:T(4,128)}, f32[4,128,64]{1,2,0:T(8,128)}) %tuple.61, (s32[1024]{0:T(1024)S(1)}, s32[128]{0:T(128)S(1)}, s32[]{:T(128)}, ...), branch_computations={%region_4.3_spmd, %region_5.6_spmd} | conditional | flops 176358400 | bytes 11080266 | solution.py:100
  286.0 1.9 constant_dynamic-slice_fusion
  289.4 1.3 multiply_add_fusion
  290.6 2.2 convolution_add_fusion
  295.9 6.9 %conditional.4 = ((f32[4,128]{1,0:T(4,128)S(1)}, f32[4,128]{1,0:T(4,128)}, f32[4,128,64]{1,2,0:T(8,128)})) conditional(s32[]{:T(128)} %convert_element_type.152, (f32[4,128]{1,0:T(4,128)S(1)}, f32[4,128]{1,0:T(4,128)}, f32[4,128,64]{1,2,0:T(8,128)}) %tuple.61, (s32[1024]{0:T(1024)S(1)}, s32[128]{0:T(128)S(1)}, s32[]{:T(128)}, ...), branch_computations={%region_4.3_spmd, %region_5.6_spmd} | conditional | flops 176358400 | bytes 11080266 | solution.py:100
  295.9 1.9 constant_dynamic-slice_fusion
  299.3 1.3 multiply_add_fusion
  300.6 2.2 convolution_add_fusion
  305.8 6.9 %conditional.4 = ((f32[4,128]{1,0:T(4,128)S(1)}, f32[4,128]{1,0:T(4,128)}, f32[4,128,64]{1,2,0:T(8,128)})) conditional(s32[]{:T(128)} %convert_element_type.152, (f32[4,128]{1,0:T(4,128)S(1)}, f32[4,128]{1,0:T(4,128)}, f32[4,128,64]{1,2,0:T(8,128)}) %tuple.61, (s32[1024]{0:T(1024)S(1)}, s32[128]{0:T(128)S(1)}, s32[]{:T(128)}, ...), branch_computations={%region_4.3_spmd, %region_5.6_spmd} | conditional | flops 176358400 | bytes 11080266 | solution.py:100
  305.8 1.9 constant_dynamic-slice_fusion
  309.2 1.3 multiply_add_fusion
  310.5 2.2 convolution_add_fusion
  315.7 6.9 %conditional.4 = ((f32[4,128]{1,0:T(4,128)S(1)}, f32[4,128]{1,0:T(4,128)}, f32[4,128,64]{1,2,0:T(8,128)})) conditional(s32[]{:T(128)} %convert_element_type.152, (f32[4,128]{1,0:T(4,128)S(1)}, f32[4,128]{1,0:T(4,128)}, f32[4,128,64]{1,2,0:T(8,128)}) %tuple.61, (s32[1024]{0:T(1024)S(1)}, s32[128]{0:T(128)S(1)}, s32[]{:T(128)}, ...), branch_computations={%region_4.3_spmd, %region_5.6_spmd} | conditional | flops 176358400 | bytes 11080266 | solution.py:100
  315.8 1.9 constant_dynamic-slice_fusion
  319.1 1.3 multiply_add_fusion
  320.4 2.2 convolution_add_fusion
  325.7 6.9 %conditional.4 = ((f32[4,128]{1,0:T(4,128)S(1)}, f32[4,128]{1,0:T(4,128)}, f32[4,128,64]{1,2,0:T(8,128)})) conditional(s32[]{:T(128)} %convert_element_type.152, (f32[4,128]{1,0:T(4,128)S(1)}, f32[4,128]{1,0:T(4,128)}, f32[4,128,64]{1,2,0:T(8,128)}) %tuple.61, (s32[1024]{0:T(1024)S(1)}, s32[128]{0:T(128)S(1)}, s32[]{:T(128)}, ...), branch_computations={%region_4.3_spmd, %region_5.6_spmd} | conditional | flops 176358400 | bytes 11080266 | solution.py:100
  325.7 1.8 constant_dynamic-slice_fusion
  329.0 1.3 multiply_add_fusion
  330.3 2.2 convolution_add_fusion
  332.6 0.9 fusion.41
  333.6 0.8 convert_element_type.100
  334.4 3.3 all-to-all-start
  337.7 2.2 multiply_reduce_fusion
  339.9 3.4 all-to-all-done
  343.3 3.8 %convolution_convert_fusion.2 = bf16[32,2048]{1,0:T(8,128)(2,1)} fusion(bf16[32,1024]{1,0:T(8,128)(2,1)S(1)} %bitcast.60, bf16[1024,2048]{1,0:T(8,128)(2,1)} %param.27), kind=kOutput, calls=%fused_computation.29 | convolution fusion | flops 134283264 | bytes 4390912 | tf_op jit(solution)/shard_map/dot_general | solution.py:152
  (147 shorter events, 26.8 us)
Async XLA Ops:
  7.2 121.6 %copy-start = (bf16[1,256,2048]{2,1,0:T(8,128)(2,1)S(1)}, bf16[1,256,2048]{2,1,0:T(8,128)(2,1)}, u32[]{:S(2)}) copy-start(bf16[1,256,2048]{2,1,0:T(8,128)(2,1)} %param.35) | copy-start | bytes 3145732
  7.2 20.2 %copy-start.3 = (bf16[64,2048]{1,0:T(8,128)(2,1)S(1)}, bf16[64,2048]{1,0:T(8,128)(2,1)}, u32[]{:S(2)}) copy-start(bf16[64,2048]{1,0:T(8,128)(2,1)} %param.28) | copy-start | bytes 786436
  7.2 20.4 %copy-start.5 = (f32[2048]{0:T(1024)S(1)}, f32[2048]{0:T(1024)}, u32[]{:S(2)}) copy-start(f32[2048]{0:T(1024)} %param.29) | copy-start | bytes 24580
  7.2 224.0 %all-gather.2.cloned.1.call-start = ((), (), s32[]{:S(2)}) async-start(), calls=%async_computation.5 | async-start | bytes 10649600 | tf_op jit(solution)/shard_map/all_gather | solution.py:17
  72.8 54.8 %copy-start.8 = (bf16[1,2048,256]{2,1,0:T(8,128)(2,1)S(1)}, bf16[1,2048,256]{2,1,0:T(8,128)(2,1)}, u32[]{:S(2)}) copy-start(bf16[1,2048,256]{2,1,0:T(8,128)(2,1)} %param.33) | copy-start | bytes 3145732
  125.6 2.0 copy-start.2
  127.5 1.3 copy-start.9
  194.6 7.8 %copy-start.4 = (bf16[128,384]{1,0:T(8,128)(2,1)S(1)}, bf16[128,384]{1,0:T(8,128)(2,1)}, u32[]{:S(2)}) copy-start(bf16[128,384]{1,0:T(8,128)(2,1)} %param.21) | copy-start | bytes 294916
  194.6 8.1 %copy-start.6 = (f32[64,2]{0,1:T(2,128)S(1)}, f32[64,2]{0,1:T(2,128)}, u32[]{:S(2)}) copy-start(f32[64,2]{0,1:T(2,128)} %param.32) | copy-start | bytes 1540
  194.6 8.1 %copy-start.7 = (f32[64]{0:T(128)S(1)}, f32[64]{0:T(128)}, u32[]{:S(2)}) copy-start(f32[64]{0:T(128)} %param.31) | copy-start | bytes 772
  195.8 33.5 %all-to-all-start.4 = ((bf16[64,4,2048]{2,1,0:T(4,128)(2,1)}), bf16[64,4,2048]{2,1,0:T(4,128)(2,1)S(1)}, u32[]{:S(2)}, u32[]{:S(2)}) async-start(bf16[64,4,2048]{2,1,0:T(4,128)(2,1)} %reshape.214), calls=%async_computation.4 | async-start | bytes 2097152 | tf_op jit(solution)/shard_map/all_to_all | solution.py:193
  334.4 8.9 %all-to-all-start = ((bf16[4,32,256]{2,1,0:T(8,128)(2,1)}), bf16[4,32,256]{2,1,0:T(8,128)(2,1)S(1)}, u32[]{:S(2)}, u32[]{:S(2)}) async-start(bf16[4,32,256]{2,1,0:T(8,128)(2,1)} %convert_element_type.100), calls=%async_computation | async-start | bytes 131072 | tf_op jit(solution)/shard_map/all_to_all | solution.py:151
  343.3 3.8 %copy-start.1 = (bf16[1,256,2048]{2,1,0:T(8,128)(2,1)S(1)}, bf16[1,256,2048]{2,1,0:T(8,128)(2,1)}, u32[]{:S(2)}) copy-start(bf16[1,256,2048]{2,1,0:T(8,128)(2,1)} %param.35) | copy-start | bytes 3145732
Sparse Core Ops, SparseCore 0:
  25.8 88.9 all-gather.1
